TPU v7x, 32 devices: a whole 2x2x4 slice. The times are simulated.
32 devices in a mesh: sp: 8 (over z, y), tp: 4 (over x, core).
Axes of the slice: x: 2, y: 2, z: 4, core: 2. Of those that a mesh axis runs over, the one named last changes fastest.
Arguments:
- queries: bfloat16 [4096, 1024], P('sp', 'tp'), may hold values from -6 to 6
- keys: bfloat16 [4096, 1024], P('sp', 'tp'), may hold values from -6 to 6
- values: bfloat16 [4096, 1024], P('sp', 'tp'), may hold values from -6 to 6
- output_gate_logits: bfloat16 [4096, 1024], P('sp', 'tp'), may hold values from -6 to 6
- input_gate_log: float32 [4096, 8], P('sp', 'tp'), may hold values from -5 to 125
- forget_gate_logits: float32 [4096, 8], P('sp', 'tp')
- extra_decay_log: float32 [4096, 8], P('sp', 'tp'), may hold values from -1 to 0
- document: int32 [4096], P('sp'), may hold values from 0 to 3, never falling along the last dimension, each value on 1 to 2048 neighbouring positions
- residual: bfloat16 [4096, 2048], P('sp', 'tp'), may hold values from -16 to 16
- cell_norm_gain: bfloat16 [1024], P('tp'), may hold values from 0.099609375 to 1.8984375
- output_weight: bfloat16 [1024, 2048], P('tp'), may hold values from -0.1875 to 0.1875
- mixer_norm_gain: bfloat16 [2048], P('tp'), may hold values from 0.099609375 to 1.8984375
- up_weight: bfloat16 [2048, 8192], P('sp', 'tp'), may hold values from -0.125 to 0.125
- down_weight: bfloat16 [8192, 2048], P('tp', 'sp'), may hold values from -0.0625 to 0.0625
Outputs:
- layer_out: bfloat16 [4096, 2048], P('sp', 'tp')
All inputs are finite; a program needn't handle non-finite values.
Results may differ from a plain program's by a relative error of at most 0.015.
Values may be sent and summed in bfloat16 or wider, within the bound.
A program may use at most 128 MiB of HBM per device.

v0:
```python
import jax
import jax.numpy as jnp
from jax import lax
from jax.sharding import PartitionSpec as P

DH = 128
BLOCK = 128


NEG = -1e30
EPS = 1e-06
HIGH = lax.Precision.HIGHEST


def carried_in(value, axis, join, neutral):
    count, mine = (lax.axis_size(axis), lax.axis_index(axis))
    pieces = jax.tree.map(lambda part: lax.all_gather(part, axis), value)
    subtotal = jax.tree.map(
        lambda part, zero: jnp.full_like(part, 0) + jnp.asarray(zero, part.dtype), value, neutral
    )

    def step(position, subtotal):
        longer = join(subtotal, jax.tree.map(lambda part: part[position], pieces))
        return jax.tree.map(lambda new, old: jnp.where(position < mine, new, old), longer, subtotal)

    return lax.fori_loop(0, count - 1, step, subtotal)


def block_terms(carry, inputs):
    memory, normer, stabil, last_doc = carry
    q_blk, k_blk, v_blk, gate_in, gate_log, doc_blk = inputs
    length = doc_blk.shape[0]
    causal = jnp.arange(length)[:, None] >= jnp.arange(length)[None, :]
    cumulative = jnp.cumsum(gate_log, axis=-1)
    same_doc = (doc_blk[:, None] == doc_blk[None, :]) & causal
    pair_log = cumulative[:, :, None] - cumulative[:, None, :] + gate_in[:, None, :]
    pair_log = jnp.where(same_doc[None], pair_log, NEG)
    live_rows = doc_blk == last_doc
    carried_log = jnp.where(live_rows[None, :], cumulative + stabil[:, None], NEG)
    peak_log = jnp.maximum(carried_log, jnp.max(pair_log, axis=-1))
    weights = jnp.exp(pair_log - peak_log[:, :, None])
    carried = jnp.exp(carried_log - peak_log)
    scores = jnp.einsum("htd,hsd->hts", q_blk, k_blk, precision=HIGH) * weights
    numerator = carried[:, :, None] * jnp.einsum("htd,hde->hte", q_blk, memory, precision=HIGH)
    numerator = numerator + jnp.einsum("hts,hse->hte", scores, v_blk, precision=HIGH)
    denominator = carried * jnp.einsum("htd,hd->ht", q_blk, normer, precision=HIGH) + jnp.sum(
        scores, axis=-1
    )
    end_doc = doc_blk[-1]
    end_cum = cumulative[:, -1]
    keep_log = jnp.where(
        (doc_blk == end_doc)[None, :], end_cum[:, None] - cumulative + gate_in, NEG
    )
    old_log = jnp.where(last_doc == end_doc, end_cum + stabil, NEG)
    new_stab = jnp.maximum(old_log, jnp.max(keep_log, axis=-1))
    scaled = jnp.exp(keep_log - new_stab[:, None])
    decayed = jnp.exp(old_log - new_stab)
    memory = decayed[:, None, None] * memory + jnp.einsum(
        "hs,hsd,hse->hde", scaled, k_blk, v_blk, precision=HIGH
    )
    normer = decayed[:, None] * normer + jnp.einsum("hs,hsd->hd", scaled, k_blk, precision=HIGH)
    return ((memory, normer, new_stab, end_doc), (numerator, denominator, peak_log, cumulative))


def split_heads(source, blocks):
    return source.astype(jnp.float32).reshape(blocks, BLOCK, -1, DH).transpose(0, 2, 1, 3)


def split_gates(source, blocks):
    return source.reshape(blocks, BLOCK, -1).transpose(0, 2, 1)


def within_block_pass(
    queries, keys, values, input_gate_log, forget_gate_logits, extra_decay_log, document
):
    blocks = queries.shape[0] // BLOCK
    head_count = queries.shape[1] // DH
    query_heads = split_heads(queries, blocks) * DH ** (-0.5)
    forget_log_values = jax.nn.log_sigmoid(forget_gate_logits) + extra_decay_log
    inputs = (
        query_heads,
        split_heads(keys, blocks),
        split_heads(values, blocks),
        split_gates(input_gate_log, blocks),
        split_gates(forget_log_values, blocks),
        document.reshape(blocks, BLOCK),
    )
    initial = (
        jnp.zeros((head_count, DH, DH), jnp.float32),
        jnp.zeros((head_count, DH), jnp.float32),
        jnp.full((head_count,), NEG, jnp.float32),
        jnp.array(-1, jnp.int32),
    )
    final_state, output_rows = lax.scan(block_terms, initial, inputs)
    return (query_heads, final_state, output_rows)


def head_mix(cell_out, output_gate_logits, cell_norm_gain):
    row_count = output_gate_logits.shape[0]
    head_count = cell_out.shape[1]
    hidden = cell_out.transpose(0, 2, 1, 3).reshape(row_count, head_count * DH)
    squares = lax.psum(jnp.sum(hidden * hidden, axis=1), "tp")
    inverse = lax.rsqrt(squares / (head_count * DH * lax.axis_size("tp")) + EPS)
    gated = jax.nn.sigmoid(output_gate_logits.astype(jnp.float32))
    gains = cell_norm_gain.astype(jnp.float32)
    return (gated * hidden * inverse[:, None] * gains[None, :]).astype(jnp.bfloat16)


def join_states(earlier, later):
    mem_a, norm_a, stab_a, log_a, first_a, last_a = earlier
    mem_b, norm_b, stab_b, log_b, first_b, last_b = later
    joined = last_a == last_b
    stab_ab = jnp.where(joined, jnp.maximum(log_b + stab_a, stab_b), stab_b)
    weight_a = jnp.where(joined, jnp.exp(log_b + stab_a - stab_ab), 0.0)
    weight_b = jnp.exp(stab_b - stab_ab)
    memory = weight_a[:, None, None] * mem_a + weight_b[:, None, None] * mem_b
    normer = weight_a[:, None] * norm_a + weight_b[:, None] * norm_b
    blank_b = last_b < 0
    memory = jnp.where(blank_b, mem_a, memory)
    normer = jnp.where(blank_b, norm_a, normer)
    stabil = jnp.where(blank_b, stab_a, stab_ab)
    first_doc = jnp.where(first_a < 0, first_b, first_a)
    last_doc = jnp.where(blank_b, last_a, last_b)
    return (memory, normer, stabil, log_a + log_b, first_doc, last_doc)


def local(
    queries,
    keys,
    values,
    output_gate_logits,
    input_gate_log,
    forget_gate_logits,
    extra_decay_log,
    document,
    residual,
    cell_norm_gain,
    output_weight,
    mixer_norm_gain,
    up_weight,
    down_weight,
):
    query_heads, final_state, output_rows = within_block_pass(
        queries, keys, values, input_gate_log, forget_gate_logits, extra_decay_log, document
    )
    numerator, denominator, peak_log, cumulative = output_rows
    memory, normer, stabil, last_doc = final_state
    step_logs = cumulative[:, :, -1]
    offsets = jnp.cumsum(step_logs, axis=0) - step_logs
    through = cumulative + offsets[:, :, None]
    summary = (memory, normer, stabil, jnp.sum(step_logs, axis=0), document[0], last_doc)
    identity = (
        jnp.zeros_like(memory),
        jnp.zeros_like(normer),
        jnp.full_like(stabil, NEG),
        jnp.zeros_like(stabil),
        jnp.array(-1, jnp.int32),
        jnp.array(-1, jnp.int32),
    )
    prefix = carried_in(summary, "sp", join_states, identity)
    doc_blocks = document.reshape(-1, BLOCK)
    carried_log = jnp.where(
        (doc_blocks == prefix[5])[:, None, :], through + prefix[2][None, :, None], NEG
    )
    merged_peak = jnp.maximum(peak_log, carried_log)
    own_weight = jnp.exp(peak_log - merged_peak)
    far_weight = jnp.exp(carried_log - merged_peak)
    numerator = own_weight[..., None] * numerator + far_weight[..., None] * jnp.einsum(
        "nhtd,hde->nhte", query_heads, prefix[0], precision=HIGH
    )
    denominator = own_weight * denominator + far_weight * jnp.einsum(
        "nhtd,hd->nht", query_heads, prefix[1], precision=HIGH
    )
    cell_out = numerator / jnp.maximum(jnp.abs(denominator), 1.0)[..., None]
    mixed = head_mix(cell_out, output_gate_logits, cell_norm_gain)
    head_terms = jnp.dot(mixed, output_weight, preferred_element_type=jnp.float32)
    width = residual.shape[1]
    model_width = width * lax.axis_size("tp")
    own_sum = lax.psum_scatter(
        head_terms.astype(jnp.bfloat16), "tp", scatter_dimension=1, tiled=True
    ).astype(jnp.float32)
    first_sum = (residual.astype(jnp.float32) + own_sum).astype(jnp.bfloat16)
    first_wide = lax.optimization_barrier(first_sum).astype(jnp.float32)
    squares = lax.psum(jnp.sum(first_wide * first_wide, axis=1), "tp")
    inverse = lax.rsqrt(squares / model_width + EPS)
    normed_own = (first_wide * inverse[:, None] * mixer_norm_gain.astype(jnp.float32)).astype(
        jnp.bfloat16
    )
    normed_full = lax.all_gather(normed_own, "tp", axis=1, tiled=True)
    hidden = jnp.dot(
        normed_full,
        lax.all_gather(up_weight, "sp", axis=0, tiled=True),
        preferred_element_type=jnp.float32,
    )
    squared = jnp.square(jax.nn.relu(hidden)).astype(jnp.bfloat16)
    channel = jnp.dot(
        squared,
        lax.all_gather(down_weight, "sp", axis=1, tiled=True),
        preferred_element_type=jnp.float32,
    )
    own_channel = lax.psum_scatter(
        channel.astype(jnp.bfloat16), "tp", scatter_dimension=1, tiled=True
    ).astype(jnp.float32)
    return (lax.optimization_barrier(first_sum).astype(jnp.float32) + own_channel).astype(
        jnp.bfloat16
    )


def solution(mesh):
    in_specs = (
        P("sp", "tp"),
        P("sp", "tp"),
        P("sp", "tp"),
        P("sp", "tp"),
        P("sp", "tp"),
        P("sp", "tp"),
        P("sp", "tp"),
        P("sp"),
        P("sp", "tp"),
        P("tp"),
        P("tp", None),
        P("tp"),
        P("sp", "tp"),
        P("tp", "sp"),
    )
    out_specs = P("sp", "tp")
    return jax.shard_map(local, mesh=mesh, in_specs=in_specs, out_specs=out_specs, check_vma=False)
```

profile of v0, /device:TPU:23, one launch (start us, length us, event | category | flops | bytes accessed | tf_op | source)
XLA Modules:
  0.0 498.6 jit_solution(16988237167681294159)
XLA Ops:
  6.6 1.1 convert_multiply_fusion.2
  7.9 1.2 reshape.228
  9.1 1.2 reshape.229
  10.4 0.7 fusion.41
  11.1 32.2 %while.45 = (s32[]{:T(128)}, f32[2,128,128]{2,1,0:T(8,128)S(1)}, f32[2,128]{1,0:T(2,128)S(1)}, f32[2]{0:T(128)S(1)}, s32[]{:T(128)}, /*index=5*/f32[4,2,128,128]...) while((s32[]{:T(128)}, f32[2,128,128]{2,1,0:T(8,128)S(1)}, ...), condition=%wide.region_5.6_spmd.clone, body=%wide.region_0.5_spmd.clone.sunk | while | flops 202756624 | bytes 3500908 | solution.py:94
  11.6 0.7 compare_bitcast_fusion.4
  14.2 0.9 fusion.84
  17.9 0.7 constant_dynamic-update-slice_fusion.7
  19.7 0.7 compare_bitcast_fusion.4
  22.2 0.9 fusion.84
  25.9 0.7 constant_dynamic-update-slice_fusion.7
  27.7 0.7 compare_bitcast_fusion.4
  30.3 0.9 fusion.84
  33.9 0.7 constant_dynamic-update-slice_fusion.7
  35.8 0.7 compare_bitcast_fusion.4
  38.3 0.9 fusion.84
  42.0 0.7 constant_dynamic-update-slice_fusion.7
  45.3 0.7 dynamic-update-slice
  46.6 6.5 %all-reduce = s32[8]{0:T(128)S(1)} all-reduce(s32[8]{0:T(128)S(1)} %dynamic-update-slice), channel_id=1, replica_groups=mesh['sp'=8,'tp'=4] {'sp'}, use_global_device_ids=true, to_apply=%add | all-reduce | flops 8 | bytes 64
  53.1 11.8 %all-reduce.3 = (f32[16]{0:T(128)S(1)}, f32[16]{0:T(128)S(1)}) all-reduce(f32[16]{0:T(128)S(1)} %dynamic-update-slice.1, f32[16]{0:T(128)S(1)} %dynamic-update-slice.2), channel_id=2, replica_groups=mesh['sp'=8,'tp'=4] {'sp'}, use_global_device_ids=true, to_apply=%add.1 | all-reduce | flops 32 | bytes 256
  65.5 14.9 %all-gather.4 = f32[8,2,128]{2,1,0:T(2,128)S(1)} all-gather(f32[1,2,128]{2,1,0:T(2,128)S(1)} %bitcast.220), channel_id=5, replica_groups=mesh['sp'=8,'tp'=4] {'sp'}, dimensions={0}, use_global_device_ids=true | all-gather | bytes 9216 | tf_op jit(solution)/shard_map/all_gather | solution.py:17
  80.4 1.7 all-gather.16.cloned.1.call-done
  82.2 27.4 %while.46 = (s32[]{:T(128)}, f32[2,128,128]{2,1,0:T(8,128)S(1)}, f32[2,128]{1,0:T(2,128)S(1)}, f32[2]{0:T(128)S(1)}, s32[]{:T(128)}, /*index=5*/s32[]{:T(128)}, ...) while((s32[]{:T(128)}, f32[2,128,128]{2,1,0:T(8,128)S(1)}, ...), condition=%wide.region_8.9_spmd.clone, body=%wide.region_7.8_spmd.clone.sunk | while | flops 198174 | bytes 396667 | solution.py:26
  85.1 1.0 select_select_fusion.4
  86.1 0.7 dynamic_slice.112
  89.0 1.0 select_select_fusion.4
  90.0 0.7 dynamic_slice.112
  92.9 1.0 select_select_fusion.4
  93.9 0.7 dynamic_slice.112
  96.8 1.0 select_select_fusion.4
  97.8 0.7 dynamic_slice.112
  100.7 1.0 select_select_fusion.4
  104.6 1.0 select_select_fusion.4
  108.5 1.0 select_select_fusion.4
  109.5 0.7 broadcast_compare_fusion
  110.7 0.7 multiply_reduce_fusion
  111.5 13.5 %psum.14 = f32[512]{0:T(512)S(1)} all-reduce(f32[512]{0:T(512)S(1)} %bitcast.225), channel_id=1, replica_groups=mesh['sp'=8,'tp'=4] {'tp'}, use_global_device_ids=true, to_apply=%region_11.12 | all-reduce | flops 512 | bytes 4096 | tf_op jit(solution)/shard_map/psum | solution.py:102
  125.2 2.1 convolution_convert_fusion
  127.5 33.2 %reduce-scatter.3.cloned.1.call-done = bf16[512,512]{1,0:T(8,128)(2,1)} async-done(((bf16[512,2048]{1,0:T(8,128)(2,1)}), bf16[512,512]{1,0:T(8,128)(2,1)}) %reduce-scatter.3.cloned.1.call-update) | async-done | bytes 524304 | tf_op jit(solution)/shard_map/reduce_scatter | solution.py:179
  160.6 1.2 add_convert_fusion
  162.0 5.8 %psum.15 = f32[512]{0:T(512)S(1)} all-reduce(f32[512]{0:T(512)S(1)} %fusion.25), channel_id=1, replica_groups=mesh['sp'=8,'tp'=4] {'tp'}, use_global_device_ids=true, to_apply=%region_14.15 | all-reduce | flops 512 | bytes 4096 | tf_op jit(solution)/shard_map/psum | solution.py:184
  167.9 1.0 fusion.27
  170.3 22.4 %all-gather.10.cloned.1.call-done = bf16[512,2048]{1,0:T(8,128)(2,1)} async-done(((bf16[512,512]{1,0:T(8,128)(2,1)}), bf16[512,2048]{1,0:T(8,128)(2,1)}) %all-gather.10.cloned.1.call-update) | async-done | bytes 2097168 | tf_op jit(solution)/shard_map/all_gather | solution.py:189
  192.7 124.5 %all-gather.12.cloned.1.call-done = bf16[2048,2048]{1,0:T(8,128)(2,1)} async-done(((bf16[256,2048]{1,0:T(8,128)(2,1)}), bf16[2048,2048]{1,0:T(8,128)(2,1)}) %all-gather.12.cloned.1.call-update) | async-done | bytes 8388624 | tf_op jit(solution)/shard_map/all_gather | solution.py:192
  317.2 125.0 %all-gather.14.cloned.1.call-done = bf16[2048,2048]{1,0:T(8,128)(2,1)} async-done(((bf16[2048,256]{1,0:T(8,128)(2,1)}), bf16[2048,2048]{1,0:T(8,128)(2,1)}) %all-gather.14.cloned.1.call-update) | async-done | bytes 8388624 | tf_op jit(solution)/shard_map/all_gather | solution.py:198
  442.2 16.5 %convolution_convert_fusion.1 = bf16[512,2048]{1,0:T(8,128)(2,1)} fusion(bf16[2048,2048]{1,0:T(8,128)(2,1)} %all-gather.14.cloned.1.call-done, bf16[512,2048]{1,0:T(8,128)(2,1)} %all-gather.10.cloned.1.call-done, bf16[2048,2048]{1,0:T(8,128)(2,1)} %all-gather.12.cloned.1.call-done), kind=kOutput, calls=%fused_computation.68 | convolution fusion | flops 8594128896 | bytes 20971520 | tf_op jit(solution)/shard_map/dot_general | solution.py:196
  458.8 31.0 %reduce-scatter.5.cloned.1.call-done = bf16[512,512]{1,0:T(8,128)(2,1)} async-done(((bf16[512,2048]{1,0:T(8,128)(2,1)}), bf16[512,512]{1,0:T(8,128)(2,1)}) %reduce-scatter.5.cloned.1.call-update) | async-done | bytes 524304 | tf_op jit(solution)/shard_map/reduce_scatter | solution.py:201
  489.8 2.0 fusion.28
  (174 shorter events, 26.0 us)
Async XLA Ops:
  6.5 118.7 %copy-start = (bf16[256,2048]{1,0:T(8,128)(2,1)S(1)}, bf16[256,2048]{1,0:T(8,128)(2,1)}, u32[]{:S(2)}) copy-start(bf16[256,2048]{1,0:T(8,128)(2,1)} %param.28) | copy-start | bytes 3145732
  6.5 75.6 %all-gather.16.cloned.1.call-start = ((), (), s32[]{:S(2)}) async-start(), calls=%async_computation.7 | async-start | bytes 1179648 | tf_op jit(solution)/shard_map/all_gather | solution.py:17
  11.1 32.9 %copy-start.7 = (u32[32]{0:T(128)S(1)}, u32[32]{0:T(128)}, u32[]{:S(2)}) copy-start(u32[32]{0:T(128)} %constant.102) | copy-start | bytes 388
  11.1 54.0 %copy-start.6 = (bf16[256]{0:T(256)(128)(2,1)S(1)}, bf16[256]{0:T(256)(128)(2,1)}, u32[]{:S(2)}) copy-start(bf16[256]{0:T(256)(128)(2,1)} %param.27) | copy-start | bytes 1540
  43.3 0.6 copy-start.1
  43.3 67.4 %copy-start.4 = (f32[4,2,128,128]{2,3,0,1:T(8,128)S(1)}, f32[4,2,128,128]{2,3,0,1:T(8,128)}, u32[]{:S(2)}) copy-start(f32[4,2,128,128]{2,3,0,1:T(8,128)} %get-tuple-element.284) | copy-start | bytes 1572868
  43.3 81.9 %copy-start.5 = (bf16[512,256]{1,0:T(8,128)(2,1)S(1)}, bf16[512,256]{1,0:T(8,128)(2,1)}, u32[]{:S(2)}) copy-start(bf16[512,256]{1,0:T(8,128)(2,1)} %param.21) | copy-start | bytes 786436
  44.0 116.7 %reduce-scatter.3.cloned.1.call-start = ((), (), s32[]{:S(2)}) async-start(), calls=%async_computation.2 | async-start | bytes 2621440 | tf_op jit(solution)/shard_map/reduce_scatter | solution.py:179
  111.5 16.0 %copy-start.3 = (bf16[512]{0:T(512)(128)(2,1)S(1)}, bf16[512]{0:T(512)(128)(2,1)}, u32[]{:S(2)}) copy-start(bf16[512]{0:T(512)(128)(2,1)} %param.29) | copy-start | bytes 3076
  111.5 49.2 %copy-start.2 = (bf16[512,512]{1,0:T(8,128)(2,1)S(1)}, bf16[512,512]{1,0:T(8,128)(2,1)}, u32[]{:S(2)}) copy-start(bf16[512,512]{1,0:T(8,128)(2,1)} %param.26) | copy-start | bytes 1572868
  127.4 65.3 %all-gather.10.cloned.1.call-start = ((), (), s32[]{:S(2)}) async-start(), calls=%async_computation.3 | async-start | bytes 2621440 | tf_op jit(solution)/shard_map/all_gather | solution.py:189
  168.9 148.3 %all-gather.12.cloned.1.call-start = ((), (), s32[]{:S(2)}) async-start(), calls=%async_computation.4 | async-start | bytes 9437184 | tf_op jit(solution)/shard_map/all_gather | solution.py:192
  169.5 272.7 %all-gather.14.cloned.1.call-start = ((), (), s32[]{:S(2)}) async-start(), calls=%async_computation.5 | async-start | bytes 9437184 | tf_op jit(solution)/shard_map/all_gather | solution.py:198
  170.1 319.7 %reduce-scatter.5.cloned.1.call-start = ((), (), s32[]{:S(2)}) async-start(), calls=%async_computation.6 | async-start | bytes 2621440 | tf_op jit(solution)/shard_map/reduce_scatter | solution.py:201
Sparse Core Ops, SparseCore 0:
  44.1 38.0 all-gather.15
  127.5 33.0 reduce-scatter.2
  169.0 23.6 all-gather.9
  194.7 122.4 all-gather.11
  319.1 123.1 all-gather.13
  458.9 30.8 reduce-scatter.4
where the time goes:
time: 502 us; the launch traced here: 499 us
  waiting for transfers between devices  339 us (68%)
  blocking collectives  52.4 us (10%)
  matrix products  28.2 us (6%)
  other arithmetic  27 us (5%)
  loops' own time  20.3 us (4%)
  local copies, waits for them, and re-layouts  17 us (3%)
  between operations  14.4 us (3%)
    all_gather x1, waiting for transfers between devices, local(): lax.all_gather(down_weight, 'sp', axis=1, tiled=True)  125 us
    all_gather x1, waiting for transfers between devices, local(): lax.all_gather(up_weight, 'sp', axis=0, tiled=True)  124 us
    reduce_scatter x1, waiting for transfers between devices, local(): lax.psum_scatter(head_terms.astype(jnp.bfloat16), 'tp', scatter_dimension...  33.2 us
    reduce_scatter x1, waiting for transfers between devices, local(): lax.psum_scatter(channel.astype(jnp.bfloat16), 'tp', scatter_dimension=1,...  31 us
    all_gather x1, waiting for transfers between devices, local(): normed_full = lax.all_gather(normed_own, 'tp', axis=1, tiled=True)  22.4 us
    unnamed x2, blocking collectives  18.2 us
    dot_general x1, matrix products, local(): jnp.dot(squared, lax.all_gather(down_weight, 'sp', axis=1, tiled=True), p...  16.5 us
    another operation x1, loops' own time, carried_in(): return lax.fori_loop(0, count - 1, step, subtotal)  14.9 us
  transfers between devices with their start and end apart: 6, of which 6 were waited for; matrix products, arithmetic and copies ran while one was open for 1% of the time, Pallas kernels for 0%

commit v1 on v0

--- a/solution.py
+++ b/solution.py
@@ -1,10 +1,15 @@
+import functools
+
 import jax
 import jax.numpy as jnp
 from jax import lax
+from jax.experimental import pallas as pl
+from jax.experimental.pallas import tpu as pltpu
 from jax.sharding import PartitionSpec as P
 
 DH = 128
 BLOCK = 128
+MOST = 2048
 
 
 NEG = -1e30
@@ -206,6 +211,527 @@
     )
 
 
+MESH = pl.DeviceIdType.MESH
+F32 = jnp.float32
+BF16 = jnp.bfloat16
+STATE_ROWS = DH + 8
+
+
+def to_columns(rows):
+    pad = jnp.zeros((128 - rows.shape[0], rows.shape[1]), F32)
+    return jnp.transpose(jnp.concatenate([rows, pad], axis=0))
+
+
+def row_sums(wide):
+    ones = jnp.ones((8, wide.shape[1]), F32)
+    return lax.dot_general(
+        ones, wide, (((1,), (1,)), ((), ())), precision=HIGH, preferred_element_type=F32
+    )
+
+
+def layer_kernel(
+    n,
+    m,
+    back,
+    q_ref,
+    k_ref,
+    v_ref,
+    og_ref,
+    gates_ref,
+    resid_ref,
+    cgain_ref,
+    wout_ref,
+    mgain_ref,
+    up_ref,
+    down_ref,
+    out_ref,
+    up_all,
+    down_all,
+    state_out,
+    state_in,
+    y_ref,
+    terms_out,
+    terms_in,
+    squares_out,
+    squares_in,
+    first_ref,
+    normed,
+    sums_out,
+    sums_in,
+    squared,
+    parts_out,
+    parts_in,
+    ring_send,
+    ring_recv,
+    state_send,
+    state_recv,
+    terms_send,
+    terms_recv,
+    squares_send,
+    squares_recv,
+    normed_send,
+    normed_recv,
+    sums_send,
+    sums_recv,
+    parts_send,
+    parts_recv,
+):
+    sp, tp = lax.axis_index("sp"), lax.axis_index("tp")
+    rows, heads = q_ref.shape[0], q_ref.shape[1] // DH
+    depth, hidden_width = up_ref.shape
+    half, quarter = depth // 2, depth // 4
+    width = resid_ref.shape[1]
+    per_owner = width // depth
+
+    def index_of(position):
+        late = position // (n // 2)
+        return (1 - late) * 2 * position + late * (2 * (n - 1 - position) + 1)
+
+    odd = sp % 2
+    place = (1 - odd) * (sp // 2) + odd * (n - 1 - sp // 2)
+    target = (index_of((place + 1) % n), index_of((place + n - 1) % n))
+
+    barrier = pltpu.get_barrier_semaphore()
+    for k in range(1, n):
+        pl.semaphore_signal(barrier, device_id=((sp + k) % n, tp), device_id_type=MESH)
+    for k in range(1, m):
+        pl.semaphore_signal(barrier, device_id=(sp, (tp + k) % m), device_id_type=MESH)
+    pl.semaphore_wait(barrier, n + m - 2)
+
+    def block_at(way, step):
+        return index_of((place + (n - step if way == 0 else step)) % n)
+
+    def ring(stream, way, step, sub):
+        block = block_at(way, step)
+        if stream == 0:
+            inner = way * half + sub * quarter
+            where = pl.ds(pl.multiple_of(block * depth + inner, quarter), quarter)
+            dst = up_all.at[where, :]
+            src = up_ref.at[pl.ds(inner, quarter), :] if step == 0 else dst
+        else:
+            deep = pl.ds(sub * (hidden_width // 2), hidden_width // 2)
+            dst = down_all.at[block, way, deep, :]
+            src = down_ref.at[deep, pl.ds(way * half, half)] if step == 0 else dst
+        return pltpu.make_async_remote_copy(
+            src_ref=src,
+            dst_ref=dst,
+            send_sem=ring_send.at[stream, way, step, sub],
+            recv_sem=ring_recv.at[stream, way, step, sub],
+            device_id=(target[way], tp),
+            device_id_type=MESH,
+        )
+
+    def arrived(stream, way, step, sub):
+        block = block_at(way, step + 1)
+        if stream == 0:
+            inner = way * half + sub * quarter
+            dst = up_all.at[pl.ds(pl.multiple_of(block * depth + inner, quarter), quarter), :]
+        else:
+            dst = down_all.at[block, way, pl.ds(sub * (hidden_width // 2), hidden_width // 2), :]
+        pltpu.make_async_remote_copy(
+            src_ref=dst,
+            dst_ref=dst,
+            send_sem=ring_send.at[stream, way, step, sub],
+            recv_sem=ring_recv.at[stream, way, step, sub],
+            device_id=(target[way], tp),
+            device_id_type=MESH,
+        ).wait_recv()
+
+    def open_stream(stream):
+        for sub in range(2):
+            for way in range(2):
+                ring(stream, way, 0, sub).start()
+
+    events = [(a, b, c) for a in range(2) for b in range(n - 1) for c in range(2)]
+    done = [0]
+
+    def pump():
+        stream, step, sub = events[done[0]]
+        done[0] += 1
+        for way in range(2):
+            arrived(stream, way, step, sub)
+            if step + 1 < n - 1:
+                ring(stream, way, step + 1, sub).start()
+        if stream == 0 and step == n - 3 and sub == 1:
+            open_stream(1)
+
+    open_stream(0)
+
+    gates = gates_ref[...]
+    document = gates[2 * heads : 2 * heads + 1, :]
+    across = lax.broadcasted_iota(jnp.int32, (rows, rows), 1)
+    along = lax.broadcasted_iota(jnp.int32, (rows, rows), 0)
+    upper = (along <= across).astype(F32)
+    sums = jnp.dot(gates, upper, precision=HIGH, preferred_element_type=F32)
+    last_doc = document[:, rows - 1 : rows]
+    totals, stabs, scaled = [], [], []
+    for h in range(heads):
+        total = sums[h : h + 1, rows - 1 : rows]
+        keep = total - sums[h : h + 1, :] + gates[heads + h : heads + h + 1, :]
+        keep = jnp.where(document == last_doc, keep, NEG)
+        stab = jnp.max(keep, axis=1, keepdims=True)
+        totals.append(total)
+        stabs.append(stab)
+        scaled.append(jnp.exp(keep - stab))
+    slab = lax.broadcasted_iota(jnp.int32, (8, rows), 0)
+    packed = jnp.broadcast_to(document, (8, rows))
+    for h in range(heads):
+        packed = jnp.where(slab == h, sums[h : h + 1, :], packed)
+        packed = jnp.where(slab == heads + h, scaled[h], packed)
+    columns = to_columns(packed)
+    doc_col = columns[:, 2 * heads : 2 * heads + 1]
+    line = lax.broadcasted_iota(jnp.int32, (8, DH), 0)
+    for h in range(heads):
+        mine = slice(h * DH, (h + 1) * DH)
+        weighted = k_ref[:, mine].astype(F32) * columns[:, heads + h : heads + h + 1]
+        state_out[h, 0:DH, :] = jnp.dot(
+            jnp.transpose(weighted),
+            v_ref[:, mine].astype(F32),
+            precision=HIGH,
+            preferred_element_type=F32,
+        )
+        tail = jnp.broadcast_to(jnp.sum(weighted, axis=0, keepdims=True), (8, DH))
+        tail = jnp.where(line == 1, stabs[h], tail)
+        tail = jnp.where(line == 2, totals[h], tail)
+        tail = jnp.where(line == 3, last_doc, tail)
+        state_out[h, DH : DH + 8, :] = tail
+
+    def state_copy(k):
+        return pltpu.make_async_remote_copy(
+            src_ref=state_out,
+            dst_ref=state_in.at[k - 1],
+            send_sem=state_send.at[k - 1],
+            recv_sem=state_recv.at[k - 1],
+            device_id=((sp + k) % n, tp),
+            device_id_type=MESH,
+        )
+
+    for k in range(1, back + 1):
+        state_copy(k).start()
+
+    own_rows = pl.ds(pl.multiple_of(sp * depth, depth), depth)
+    up_all[own_rows, :] = up_ref[...]
+    down_all[sp, 0] = down_ref[:, 0:half]
+    down_all[sp, 1] = down_ref[:, half:depth]
+    pump()
+
+    locals_of = []
+    for h in range(heads):
+        mine = slice(h * DH, (h + 1) * DH)
+        scores = lax.dot_general(
+            q_ref[:, mine],
+            k_ref[:, mine],
+            (((1,), (1,)), ((), ())),
+            preferred_element_type=F32,
+        ) * (DH**-0.5)
+        pair = columns[:, h : h + 1] - sums[h : h + 1, :] + gates[heads + h : heads + h + 1, :]
+        pair = jnp.where((doc_col == document) & (along >= across), pair, NEG)
+        peak = jnp.max(pair, axis=1, keepdims=True)
+        scores = scores * jnp.exp(pair - peak)
+        numer = jnp.dot(
+            scores, v_ref[:, mine].astype(F32), precision=HIGH, preferred_element_type=F32
+        )
+        locals_of.append((peak, jnp.sum(scores, axis=1, keepdims=True), numer))
+        pump()
+
+    for k in range(1, back + 1):
+        state_copy(k).wait_recv()
+    first_doc = document[:, 0:1]
+    cells = []
+    for h in range(heads):
+        mine = slice(h * DH, (h + 1) * DH)
+        between = jnp.zeros((1, DH), F32)
+        logs, valids = [], []
+        best = jnp.full((1, DH), NEG, F32)
+        for k in range(1, back + 1):
+            tail = state_in[k - 1, h, DH : DH + 8, :]
+            far = lax.broadcasted_iota(jnp.int32, (1, DH), 1) * 0 + sp
+            valid = (tail[3:4, :] == first_doc) & (far >= k)
+            log = jnp.where(valid, between + tail[1:2, :], NEG)
+            between = between + tail[2:3, :]
+            best = jnp.maximum(best, log)
+            logs.append(log)
+            valids.append(valid)
+        memory = jnp.zeros((DH, DH), F32)
+        normer = jnp.zeros((1, DH), F32)
+        for k in range(1, back + 1):
+            weight = jnp.where(valids[k - 1], jnp.exp(logs[k - 1] - best), 0.0)
+            memory = memory + jnp.where(
+                valids[k - 1], weight * state_in[k - 1, h, 0:DH, :], 0.0
+            )
+            normer = normer + jnp.where(
+                valids[k - 1], weight * state_in[k - 1, h, DH : DH + 1, :], 0.0
+            )
+        peak, denom, numer = locals_of[h]
+        carried = jnp.where(doc_col == first_doc, columns[:, h : h + 1] + best[:, 0:1], NEG)
+        merged = jnp.maximum(peak, carried)
+        own, other = jnp.exp(peak - merged), jnp.exp(carried - merged)
+        query = q_ref[:, mine].astype(F32) * (DH**-0.5)
+        numer = own * numer + other * jnp.dot(
+            query, memory, precision=HIGH, preferred_element_type=F32
+        )
+        denom = own * denom + other * jnp.sum(query * normer, axis=1, keepdims=True)
+        cell = numer / jnp.maximum(jnp.abs(denom), 1.0)
+        cells.append(cell)
+        gated = jax.nn.sigmoid(og_ref[:, mine].astype(F32))
+        y_ref[:, mine] = (gated * cell * cgain_ref[:, mine].astype(F32)).astype(BF16)
+    total = cells[0] * cells[0]
+    for h in range(1, heads):
+        total = total + cells[h] * cells[h]
+    squares_out[...] = row_sums(total)
+
+    def to_peer(src, dst, send_sem, recv_sem, k):
+        return pltpu.make_async_remote_copy(
+            src_ref=src,
+            dst_ref=dst,
+            send_sem=send_sem.at[k - 1],
+            recv_sem=recv_sem.at[k - 1],
+            device_id=(sp, (tp + k) % m),
+            device_id_type=MESH,
+        )
+
+    def squares_copy(k):
+        return to_peer(squares_out, squares_in.at[k - 1], squares_send, squares_recv, k)
+
+    def terms_copy(k):
+        return to_peer(terms_out.at[k], terms_in.at[k - 1], terms_send, terms_recv, k)
+
+    def head_term(k):
+        owner = (tp + k) % m
+        cols = pl.ds(pl.multiple_of(owner * width, width), width)
+        return jnp.dot(y_ref[...], wout_ref[:, cols], preferred_element_type=F32).astype(BF16)
+
+    for k in range(1, m):
+        squares_copy(k).start()
+        terms_out[k] = head_term(k)
+        terms_copy(k).start()
+    own_term = head_term(0).astype(F32)
+    terms_out[0] = own_term.astype(BF16)
+    for _ in range(PUMPS_TERMS):
+        pump()
+    for k in range(1, m):
+        squares_copy(k).wait_recv()
+        terms_copy(k).wait_recv()
+    squares = squares_out[...]
+    attn = terms_out[0].astype(F32)
+    for k in range(1, m):
+        squares = squares + squares_in[k - 1]
+        attn = attn + terms_in[k - 1].astype(F32)
+    inverse = lax.rsqrt(to_columns(squares)[:, 0:1] / (heads * DH * m) + EPS)
+    first = (resid_ref[...].astype(F32) + attn * inverse).astype(BF16)
+    first_ref[...] = first
+    first = first.astype(F32)
+    here = pl.ds(pl.multiple_of(tp * width, width), width)
+    normed[:, here] = (first * mgain_ref[...].astype(F32)).astype(BF16)
+    sums_out[...] = row_sums(first * first)
+
+    def normed_copy(k):
+        return to_peer(normed.at[:, here], normed.at[:, here], normed_send, normed_recv, k)
+
+    def normed_arrival(k):
+        source = (tp + m - k) % m
+        there = normed.at[:, pl.ds(pl.multiple_of(source * width, width), width)]
+        return to_peer(there, there, normed_send, normed_recv, k)
+
+    def sums_copy(k):
+        return to_peer(sums_out, sums_in.at[k - 1], sums_send, sums_recv, k)
+
+    for k in range(1, m):
+        sums_copy(k).start()
+        normed_copy(k).start()
+    for _ in range(PUMPS_NORMED):
+        pump()
+    for k in range(1, m):
+        sums_copy(k).wait_recv()
+        normed_arrival(k).wait_recv()
+    squares = sums_out[...]
+    for k in range(1, m):
+        squares = squares + sums_in[k - 1]
+    scale = lax.rsqrt(to_columns(squares)[:, 0:1] / (width * m) + EPS)
+    while done[0] < 2 * (n - 1):
+        pump()
+
+    tile = min(hidden_width, 256)
+    chunks = hidden_width // tile
+
+    def up_chunk(c, carry):
+        cols = pl.ds(pl.multiple_of(c * tile, tile), tile)
+        raw = jnp.dot(normed[...], up_all[:, cols], preferred_element_type=F32)
+        hidden = jnp.maximum(raw * scale, 0.0)
+        squared[:, cols] = (hidden * hidden).astype(BF16)
+        return carry
+
+    lax.fori_loop(0, chunks // 2, up_chunk, 0)
+    pump()
+    lax.fori_loop(chunks // 2, chunks, up_chunk, 0)
+
+    def part_copy(way, step):
+        block = block_at(way, step)
+        owner, slot = block // per_owner, block % per_owner
+        return owner, pltpu.make_async_remote_copy(
+            src_ref=parts_out.at[block, way],
+            dst_ref=parts_in.at[tp, slot, way],
+            send_sem=parts_send.at[block, way],
+            recv_sem=parts_recv.at[tp, slot, way],
+            device_id=(sp, owner),
+            device_id_type=MESH,
+        )
+
+    def down_block(step):
+        for way in range(2):
+            block = block_at(way, step)
+            parts_out[block, way] = jnp.dot(
+                squared[...], down_all[block, way], preferred_element_type=F32
+            ).astype(BF16)
+            owner, copy = part_copy(way, step)
+
+            @pl.when(owner != tp)
+            def _():
+                copy.start()
+
+    down_block(0)
+    for step in range(1, n):
+        while done[0] < 2 * (n - 1) + 2 * step:
+            pump()
+        down_block(step)
+
+    for slot in range(per_owner):
+        for way in range(2):
+            cols = slice(slot * depth + way * half, slot * depth + (way + 1) * half)
+            total = parts_out[tp * per_owner + slot, way].astype(F32)
+            for k in range(1, m):
+                source = (tp + k) % m
+                there = parts_in.at[source, slot, way]
+                pltpu.make_async_remote_copy(
+                    src_ref=there,
+                    dst_ref=there,
+                    send_sem=parts_send.at[0, 0],
+                    recv_sem=parts_recv.at[source, slot, way],
+                    device_id=(sp, source),
+                    device_id_type=MESH,
+                ).wait_recv()
+                total = total + parts_in[source, slot, way].astype(F32)
+            out_ref[:, cols] = (first_ref[:, cols].astype(F32) + total).astype(BF16)
+
+    for stream, step, sub in events:
+        for way in range(2):
+            ring(stream, way, step, sub).wait_send()
+    for k in range(1, back + 1):
+        state_copy(k).wait_send()
+    for k in range(1, m):
+        squares_copy(k).wait_send()
+        terms_copy(k).wait_send()
+        sums_copy(k).wait_send()
+        normed_copy(k).wait_send()
+    for step in range(n):
+        for way in range(2):
+            owner, copy = part_copy(way, step)
+
+            @pl.when(owner != tp)
+            def _():
+                copy.wait_send()
+
+
+PUMPS_TERMS = 4
+PUMPS_NORMED = 4
+
+
+def fused(
+    n,
+    m,
+    queries,
+    keys,
+    values,
+    output_gate_logits,
+    input_gate_log,
+    forget_gate_logits,
+    extra_decay_log,
+    document,
+    residual,
+    cell_norm_gain,
+    output_weight,
+    mixer_norm_gain,
+    up_weight,
+    down_weight,
+):
+    rows, heads = queries.shape[0], queries.shape[1] // DH
+    depth, hidden_width = up_weight.shape
+    width = residual.shape[1]
+    back = min(n - 1, (MOST - 2) // rows + 1)
+    forget = jax.nn.log_sigmoid(forget_gate_logits) + extra_decay_log
+    gates = jnp.concatenate(
+        [forget.T, input_gate_log.T, document.astype(F32)[None, :]], axis=0
+    )
+    gates = jnp.pad(gates, ((0, 8 - gates.shape[0]), (0, 0)))
+    dma = pltpu.SemaphoreType.DMA
+    per_owner = width // depth
+    return pl.pallas_call(
+        functools.partial(layer_kernel, n, m, back),
+        out_shape=jax.ShapeDtypeStruct((rows, width), BF16),
+        in_specs=[pl.BlockSpec(memory_space=pltpu.VMEM)] * 11,
+        out_specs=pl.BlockSpec(memory_space=pltpu.VMEM),
+        scratch_shapes=[
+            pltpu.VMEM((n * depth, hidden_width), BF16),
+            pltpu.VMEM((n, 2, hidden_width, depth // 2), BF16),
+            pltpu.VMEM((heads, STATE_ROWS, DH), F32),
+            pltpu.VMEM((back, heads, STATE_ROWS, DH), F32),
+            pltpu.VMEM((rows, heads * DH), BF16),
+            pltpu.VMEM((m, rows, width), BF16),
+            pltpu.VMEM((m - 1, rows, width), BF16),
+            pltpu.VMEM((8, rows), F32),
+            pltpu.VMEM((m - 1, 8, rows), F32),
+            pltpu.VMEM((rows, width), BF16),
+            pltpu.VMEM((rows, m * width), BF16),
+            pltpu.VMEM((8, rows), F32),
+            pltpu.VMEM((m - 1, 8, rows), F32),
+            pltpu.VMEM((rows, hidden_width), BF16),
+            pltpu.VMEM((n, 2, rows, depth // 2), BF16),
+            pltpu.VMEM((m, per_owner, 2, rows, depth // 2), BF16),
+            dma((2, 2, n - 1, 2)),
+            dma((2, 2, n - 1, 2)),
+            dma((back,)),
+            dma((back,)),
+            dma((m - 1,)),
+            dma((m - 1,)),
+            dma((m - 1,)),
+            dma((m - 1,)),
+            dma((m - 1,)),
+            dma((m - 1,)),
+            dma((m - 1,)),
+            dma((m - 1,)),
+            dma((n, 2)),
+            dma((m, per_owner, 2)),
+        ],
+        compiler_params=pltpu.CompilerParams(
+            collective_id=0, has_side_effects=True, vmem_limit_bytes=60 * 1024 * 1024
+        ),
+        name="layer",
+    )(
+        queries,
+        keys,
+        values,
+        output_gate_logits,
+        gates,
+        residual,
+        cell_norm_gain[None, :],
+        output_weight,
+        mixer_norm_gain[None, :],
+        up_weight,
+        down_weight,
+    )
+
+
+def either(n, m, *args):
+    depth, hidden_width = args[12].shape
+    heads = args[0].shape[1] // DH
+    fits = depth % 256 == 0 and n % 2 == 0 and n >= 4 and n <= 16 and m >= 2
+    fits = fits and 2 * heads + 1 <= 8 and args[8].shape[1] % depth == 0
+    fits = fits and args[0].shape[0] % 128 == 0 and hidden_width % 256 == 0
+    if fits:
+        return fused(n, m, *args)
+    return local(*args)
+
+
 def solution(mesh):
     in_specs = (
         P("sp", "tp"),
@@ -224,4 +750,5 @@
         P("tp", "sp"),
     )
     out_specs = P("sp", "tp")
-    return jax.shard_map(local, mesh=mesh, in_specs=in_specs, out_specs=out_specs, check_vma=False)
+    body = functools.partial(either, mesh.shape["sp"], mesh.shape["tp"])
+    return jax.shard_map(body, mesh=mesh, in_specs=in_specs, out_specs=out_specs, check_vma=False)

time: 502 us -> 196 us (0.39)
  waiting for transfers between devices: 339 us -> 0 us
  Pallas kernels: 0 us -> 190 us
  blocking collectives: 52.4 us -> 0 us
  matrix products: 28.2 us -> 0 us
  other arithmetic: 27 us -> 0.64 us
  loops' own time: 20.3 us -> 0 us
  between operations: 14.4 us -> 0.03 us
  local copies, waits for them, and re-layouts: 17 us -> 4.47 us
    all_gather x4 -> x0, waiting for transfers between devices: 274 us -> none  [the longest x1 125 us: local(): lax.all_gather(down_weight, 'sp', axis=1, tiled=True)]
    pallas_call x0 -> x1, Pallas kernels: none -> 190 us  [fused(): pl.pallas_call(functools.partial(layer_kernel, n, m, back), out_shape=jax...]
    reduce_scatter x2 -> x0, waiting for transfers between devices: 64.2 us -> none  [the longest x1 33.2 us: local(): lax.psum_scatter(head_terms.astype(jnp.bfloat16), 'tp', scatter_dimension...]
    dot_general x28 -> x0, matrix products: 28.2 us -> none  [the longest x1 16.5 us: local(): jnp.dot(squared, lax.all_gather(down_weight, 'sp', axis=1, tiled=True), p...]
    another operation x2 -> x0, loops' own time: 20.3 us -> none  [the longest x1 14.9 us: carried_in(): return lax.fori_loop(0, count - 1, step, subtotal)]
    psum x2 -> x0, blocking collectives: 19.3 us -> none  [the longest x1 13.5 us: head_mix(): squares = lax.psum(jnp.sum(hidden * hidden, axis=1), 'tp')]
    unnamed x2 -> x0, blocking collectives: 18.2 us -> none
    all_gather x1 -> x0, blocking collectives: 14.9 us -> none  [carried_in(): pieces = jax.tree.map(lambda part: lax.all_gather(part, axis), value)]
  transfers between devices with their start and end apart: 6 -> 0, of which waited for: 6 -> 0; matrix products, arithmetic and copies ran while one was open for 1% -> 0% of each run, Pallas kernels for 0% -> 0%
where the time goes in v1:
time: 196 us; the launch traced here: 195 us
  Pallas kernels  190 us (97%)
  local copies, waits for them, and re-layouts  4.47 us (2%)
    pallas_call x1, Pallas kernels, fused(): pl.pallas_call(functools.partial(layer_kernel, n, m, back), out_shape=jax...  190 us

profile of v1, /device:TPU:23, one launch (start us, length us, event | category | flops | bytes accessed | tf_op | source)
XLA Modules:
  0.0 194.8 jit_solution(14363161669505000221)
XLA Ops:
  0.0 0.0 copy-start.5
  0.0 0.0 copy-start.3
  0.0 0.7 copy-done.5
  0.7 0.0 copy-start.4
  0.7 0.6 broadcast_in_dim.10.cgain_ref
  1.3 0.0 copy-done.3
  1.3 0.0 copy-start
  1.3 0.0 copy-start.1
  1.3 0.1 copy-done.4
  1.3 0.6 broadcast_in_dim.11.mgain_ref
  1.9 0.0 copy-done
  1.9 0.0 copy-done.1
  2.0 0.0 copy-start.2
  2.0 0.7 copy-done.2
  2.6 0.6 select_maximum_fusion.gates_ref
  3.3 189.6 %layer.1 = bf16[512,512]{1,0:T(8,128)(2,1)} custom-call(bf16[512,256]{1,0:T(8,128)(2,1)} %q_ref.1, bf16[512,256]{1,0:T(8,128)(2,1)} %k_ref.1, bf16[512,256]{1,0:T(8,128)(2,1)} %v_ref.1, bf16[512,256]{1,0:T(8,128)(2,1)} %og_ref.1, f32[8,512]{1,0:T(8,128)} %select_maximum_fusion.gates_ref, bf16[512,512]{1,0:T(8,128)(2,1)} %resid_ref.1, ...), custom_call_target="tpu_custom_call" | custom-call | tf_op jit(solution)/shard_map/layer/pallas_call | solution.py:668
  192.9 1.9 copy.16
  (2 shorter events, 0.0 us)
Async XLA Ops:
  0.0 0.7 copy-start.5
  0.0 1.3 copy-start.3
  0.7 0.7 copy-start.4
  1.3 0.7 copy-start
  1.3 0.7 copy-start.1
  2.0 0.7 copy-start.2

commit v2 on v1

--- a/solution.py
+++ b/solution.py
@@ -214,7 +214,6 @@
 MESH = pl.DeviceIdType.MESH
 F32 = jnp.float32
 BF16 = jnp.bfloat16
-STATE_ROWS = DH + 8
 
 
 def to_columns(rows):
@@ -239,9 +238,8 @@
     og_ref,
     gates_ref,
     resid_ref,
-    cgain_ref,
+    gain_ref,
     wout_ref,
-    mgain_ref,
     up_ref,
     down_ref,
     out_ref,
@@ -249,6 +247,8 @@
     down_all,
     state_out,
     state_in,
+    tail_out,
+    tail_in,
     y_ref,
     terms_out,
     terms_in,
@@ -265,6 +265,8 @@
     ring_recv,
     state_send,
     state_recv,
+    tail_send,
+    tail_recv,
     terms_send,
     terms_recv,
     squares_send,
@@ -337,10 +339,9 @@
             device_id_type=MESH,
         ).wait_recv()
 
-    def open_stream(stream):
-        for sub in range(2):
-            for way in range(2):
-                ring(stream, way, 0, sub).start()
+    def open_stream(stream, sub):
+        for way in range(2):
+            ring(stream, way, 0, sub).start()
 
     events = [(a, b, c) for a in range(2) for b in range(n - 1) for c in range(2)]
     done = [0]
@@ -352,10 +353,10 @@
             arrived(stream, way, step, sub)
             if step + 1 < n - 1:
                 ring(stream, way, step + 1, sub).start()
-        if stream == 0 and step == n - 3 and sub == 1:
-            open_stream(1)
-
-    open_stream(0)
+        if stream == 0 and step == n - 2:
+            open_stream(1, sub)
+
+    open_stream(0, 0)
 
     gates = gates_ref[...]
     document = gates[2 * heads : 2 * heads + 1, :]
@@ -384,30 +385,47 @@
     for h in range(heads):
         mine = slice(h * DH, (h + 1) * DH)
         weighted = k_ref[:, mine].astype(F32) * columns[:, heads + h : heads + h + 1]
-        state_out[h, 0:DH, :] = jnp.dot(
+        state_out[h] = jnp.dot(
             jnp.transpose(weighted),
             v_ref[:, mine].astype(F32),
             precision=HIGH,
             preferred_element_type=F32,
-        )
+        ).astype(BF16)
         tail = jnp.broadcast_to(jnp.sum(weighted, axis=0, keepdims=True), (8, DH))
         tail = jnp.where(line == 1, stabs[h], tail)
         tail = jnp.where(line == 2, totals[h], tail)
         tail = jnp.where(line == 3, last_doc, tail)
-        state_out[h, DH : DH + 8, :] = tail
-
-    def state_copy(k):
-        return pltpu.make_async_remote_copy(
-            src_ref=state_out,
-            dst_ref=state_in.at[k - 1],
-            send_sem=state_send.at[k - 1],
-            recv_sem=state_recv.at[k - 1],
-            device_id=((sp + k) % n, tp),
-            device_id_type=MESH,
-        )
+        tail_out[h] = tail
+
+    def state_copies(k):
+        return [
+            pltpu.make_async_remote_copy(
+                src_ref=src,
+                dst_ref=dst.at[k - 1],
+                send_sem=send_sem.at[k - 1],
+                recv_sem=recv_sem.at[k - 1],
+                device_id=((sp + k) % n, tp),
+                device_id_type=MESH,
+            )
+            for src, dst, send_sem, recv_sem in (
+                (tail_out, tail_in, tail_send, tail_recv),
+                (state_out, state_in, state_send, state_recv),
+            )
+        ]
 
     for k in range(1, back + 1):
-        state_copy(k).start()
+
+        @pl.when(sp + k < n)
+        def _():
+            for copy in state_copies(k):
+                copy.start()
+
+        @pl.when(sp < k)
+        def _():
+            tail_in[k - 1] = jnp.zeros((heads, 8, DH), F32)
+            state_in[k - 1] = jnp.zeros((heads, DH, DH), BF16)
+
+    open_stream(0, 1)
 
     own_rows = pl.ds(pl.multiple_of(sp * depth, depth), depth)
     up_all[own_rows, :] = up_ref[...]
@@ -435,7 +453,12 @@
         pump()
 
     for k in range(1, back + 1):
-        state_copy(k).wait_recv()
+
+        @pl.when(sp >= k)
+        def _():
+            for copy in state_copies(k):
+                copy.wait_recv()
+
     first_doc = document[:, 0:1]
     cells = []
     for h in range(heads):
@@ -444,7 +467,7 @@
         logs, valids = [], []
         best = jnp.full((1, DH), NEG, F32)
         for k in range(1, back + 1):
-            tail = state_in[k - 1, h, DH : DH + 8, :]
+            tail = tail_in[k - 1, h]
             far = lax.broadcasted_iota(jnp.int32, (1, DH), 1) * 0 + sp
             valid = (tail[3:4, :] == first_doc) & (far >= k)
             log = jnp.where(valid, between + tail[1:2, :], NEG)
@@ -457,10 +480,10 @@
         for k in range(1, back + 1):
             weight = jnp.where(valids[k - 1], jnp.exp(logs[k - 1] - best), 0.0)
             memory = memory + jnp.where(
-                valids[k - 1], weight * state_in[k - 1, h, 0:DH, :], 0.0
+                valids[k - 1], weight * state_in[k - 1, h].astype(F32), 0.0
             )
             normer = normer + jnp.where(
-                valids[k - 1], weight * state_in[k - 1, h, DH : DH + 1, :], 0.0
+                valids[k - 1], weight * tail_in[k - 1, h, 0:1, :], 0.0
             )
         peak, denom, numer = locals_of[h]
         carried = jnp.where(doc_col == first_doc, columns[:, h : h + 1] + best[:, 0:1], NEG)
@@ -474,7 +497,7 @@
         cell = numer / jnp.maximum(jnp.abs(denom), 1.0)
         cells.append(cell)
         gated = jax.nn.sigmoid(og_ref[:, mine].astype(F32))
-        y_ref[:, mine] = (gated * cell * cgain_ref[:, mine].astype(F32)).astype(BF16)
+        y_ref[:, mine] = (gated * cell * gain_ref[:, mine].astype(F32)).astype(BF16)
     total = cells[0] * cells[0]
     for h in range(1, heads):
         total = total + cells[h] * cells[h]
@@ -507,7 +530,7 @@
         terms_copy(k).start()
     own_term = head_term(0).astype(F32)
     terms_out[0] = own_term.astype(BF16)
-    for _ in range(PUMPS_TERMS):
+    for _ in range(min(PUMPS_TERMS, 2 * (n - 1) - done[0])):
         pump()
     for k in range(1, m):
         squares_copy(k).wait_recv()
@@ -522,7 +545,7 @@
     first_ref[...] = first
     first = first.astype(F32)
     here = pl.ds(pl.multiple_of(tp * width, width), width)
-    normed[:, here] = (first * mgain_ref[...].astype(F32)).astype(BF16)
+    normed[:, here] = (first * gain_ref[:, heads * DH :].astype(F32)).astype(BF16)
     sums_out[...] = row_sums(first * first)
 
     def normed_copy(k):
@@ -539,7 +562,7 @@
     for k in range(1, m):
         sums_copy(k).start()
         normed_copy(k).start()
-    for _ in range(PUMPS_NORMED):
+    while done[0] < 2 * (n - 1):
         pump()
     for k in range(1, m):
         sums_copy(k).wait_recv()
@@ -548,8 +571,6 @@
     for k in range(1, m):
         squares = squares + sums_in[k - 1]
     scale = lax.rsqrt(to_columns(squares)[:, 0:1] / (width * m) + EPS)
-    while done[0] < 2 * (n - 1):
-        pump()
 
     tile = min(hidden_width, 256)
     chunks = hidden_width // tile
@@ -617,7 +638,12 @@
         for way in range(2):
             ring(stream, way, step, sub).wait_send()
     for k in range(1, back + 1):
-        state_copy(k).wait_send()
+
+        @pl.when(sp + k < n)
+        def _():
+            for copy in state_copies(k):
+                copy.wait_send()
+
     for k in range(1, m):
         squares_copy(k).wait_send()
         terms_copy(k).wait_send()
@@ -632,8 +658,7 @@
                 copy.wait_send()
 
 
-PUMPS_TERMS = 4
-PUMPS_NORMED = 4
+PUMPS_TERMS = 5
 
 
 def fused(
@@ -668,13 +693,15 @@
     return pl.pallas_call(
         functools.partial(layer_kernel, n, m, back),
         out_shape=jax.ShapeDtypeStruct((rows, width), BF16),
-        in_specs=[pl.BlockSpec(memory_space=pltpu.VMEM)] * 11,
+        in_specs=[pl.BlockSpec(memory_space=pltpu.VMEM)] * 10,
         out_specs=pl.BlockSpec(memory_space=pltpu.VMEM),
         scratch_shapes=[
             pltpu.VMEM((n * depth, hidden_width), BF16),
             pltpu.VMEM((n, 2, hidden_width, depth // 2), BF16),
-            pltpu.VMEM((heads, STATE_ROWS, DH), F32),
-            pltpu.VMEM((back, heads, STATE_ROWS, DH), F32),
+            pltpu.VMEM((heads, DH, DH), BF16),
+            pltpu.VMEM((back, heads, DH, DH), BF16),
+            pltpu.VMEM((heads, 8, DH), F32),
+            pltpu.VMEM((back, heads, 8, DH), F32),
             pltpu.VMEM((rows, heads * DH), BF16),
             pltpu.VMEM((m, rows, width), BF16),
             pltpu.VMEM((m - 1, rows, width), BF16),
@@ -689,6 +716,8 @@
             pltpu.VMEM((m, per_owner, 2, rows, depth // 2), BF16),
             dma((2, 2, n - 1, 2)),
             dma((2, 2, n - 1, 2)),
+            dma((back,)),
+            dma((back,)),
             dma((back,)),
             dma((back,)),
             dma((m - 1,)),
@@ -713,9 +742,8 @@
         output_gate_logits,
         gates,
         residual,
-        cell_norm_gain[None, :],
+        jnp.concatenate([cell_norm_gain, mixer_norm_gain])[None, :],
         output_weight,
-        mixer_norm_gain[None, :],
         up_weight,
         down_weight,
     )

time: 196 us -> 187 us (0.954)
  Pallas kernels: 190 us -> 181 us
    pallas_call x1, Pallas kernels: 190 us -> 181 us  [fused(): pl.pallas_call(functools.partial(layer_kernel, n, m, back), out_shape=jax...]
where the time goes in v2:
time: 187 us; the launch traced here: 186 us
  Pallas kernels  181 us (97%)
  local copies, waits for them, and re-layouts  3.9 us (2%)
    pallas_call x1, Pallas kernels, fused(): pl.pallas_call(functools.partial(layer_kernel, n, m, back), out_shape=jax...  181 us

profile of v2, /device:TPU:23, one launch (start us, length us, event | category | flops | bytes accessed | tf_op | source)
XLA Modules:
  0.0 186.5 jit_solution(10357814967647482060)
XLA Ops:
  0.0 0.7 convert_element_type.5
  0.7 0.0 copy-start.3
  0.7 0.0 copy-start.4
  0.7 0.7 copy-done.3
  1.4 0.0 copy-done.4
  1.4 0.0 copy-start
  1.4 0.0 copy-start.1
  1.4 0.6 broadcast_in_dim.7.gain_ref
  2.0 0.1 copy-done
  2.1 0.0 copy-done.1
  2.1 0.0 copy-start.2
  2.1 0.7 copy-done.2
  2.8 0.6 select_maximum_fusion.gates_ref
  3.4 181.2 %layer.1 = bf16[512,512]{1,0:T(8,128)(2,1)} custom-call(bf16[512,256]{1,0:T(8,128)(2,1)} %q_ref.1, bf16[512,256]{1,0:T(8,128)(2,1)} %k_ref.1, bf16[512,256]{1,0:T(8,128)(2,1)} %v_ref.1, bf16[512,256]{1,0:T(8,128)(2,1)} %og_ref.1, f32[8,512]{1,0:T(8,128)} %select_maximum_fusion.gates_ref, bf16[512,512]{1,0:T(8,128)(2,1)} %resid_ref.1, ...), custom_call_target="tpu_custom_call" | custom-call | tf_op jit(solution)/shard_map/layer/pallas_call | solution.py:693
  184.6 1.9 %copy.16 = bf16[512,512]{1,0:T(8,128)(2,1)} copy(bf16[512,512]{1,0:T(8,128)(2,1)} %layer.1) | data formatting | bytes 1048576
  (2 shorter events, 0.0 us)
Async XLA Ops:
  0.7 0.7 copy-start.3
  0.7 0.7 copy-start.4
  1.4 0.7 copy-start
  1.4 0.7 copy-start.1
  2.1 0.7 copy-start.2

commit v3 on v2

--- a/solution.py
+++ b/solution.py
@@ -598,12 +598,19 @@
             device_id_type=MESH,
         )
 
-    def down_block(step):
+    middle = hidden_width // 2
+
+    def part_of(way, step, deep):
+        return jnp.dot(
+            squared[:, deep],
+            down_all[block_at(way, step), way, deep, :],
+            preferred_element_type=F32,
+        )
+
+    def down_block(step, early=(0.0, 0.0), deep=slice(0, hidden_width)):
         for way in range(2):
             block = block_at(way, step)
-            parts_out[block, way] = jnp.dot(
-                squared[...], down_all[block, way], preferred_element_type=F32
-            ).astype(BF16)
+            parts_out[block, way] = (early[way] + part_of(way, step, deep)).astype(BF16)
             owner, copy = part_copy(way, step)
 
             @pl.when(owner != tp)
@@ -611,10 +618,14 @@
                 copy.start()
 
     down_block(0)
-    for step in range(1, n):
+    for step in range(1, n - 1):
         while done[0] < 2 * (n - 1) + 2 * step:
             pump()
         down_block(step)
+    pump()
+    early = [part_of(way, n - 1, slice(0, middle)) for way in range(2)]
+    pump()
+    down_block(n - 1, early, slice(middle, hidden_width))
 
     for slot in range(per_owner):
         for way in range(2):

time: 187 us -> 187 us (level)
  no operation moved by 1% of the time
where the time goes in v3:
time: 187 us; the launch traced here: 186 us
  Pallas kernels  181 us (97%)
  local copies, waits for them, and re-layouts  3.9 us (2%)
    pallas_call x1, Pallas kernels, fused(): pl.pallas_call(functools.partial(layer_kernel, n, m, back), out_shape=jax...  181 us

profile of v3, /device:TPU:23, one launch (start us, length us, event | category | flops | bytes accessed | tf_op | source)
XLA Modules:
  0.0 186.5 jit_solution(16383480824173536290)
XLA Ops:
  0.0 0.7 convert_element_type.5
  0.7 0.0 copy-start.3
  0.7 0.0 copy-start.4
  0.7 0.7 copy-done.3
  1.4 0.0 copy-done.4
  1.4 0.0 copy-start
  1.4 0.0 copy-start.1
  1.4 0.6 broadcast_in_dim.7.gain_ref
  2.0 0.1 copy-done
  2.1 0.0 copy-done.1
  2.1 0.0 copy-start.2
  2.1 0.7 copy-done.2
  2.8 0.6 select_maximum_fusion.gates_ref
  3.4 181.2 %layer.1 = bf16[512,512]{1,0:T(8,128)(2,1)} custom-call(bf16[512,256]{1,0:T(8,128)(2,1)} %q_ref.1, bf16[512,256]{1,0:T(8,128)(2,1)} %k_ref.1, bf16[512,256]{1,0:T(8,128)(2,1)} %v_ref.1, bf16[512,256]{1,0:T(8,128)(2,1)} %og_ref.1, f32[8,512]{1,0:T(8,128)} %select_maximum_fusion.gates_ref, bf16[512,512]{1,0:T(8,128)(2,1)} %resid_ref.1, ...), custom_call_target="tpu_custom_call" | custom-call | tf_op jit(solution)/shard_map/layer/pallas_call | solution.py:704
  184.6 1.9 %copy.16 = bf16[512,512]{1,0:T(8,128)(2,1)} copy(bf16[512,512]{1,0:T(8,128)(2,1)} %layer.1) | data formatting | bytes 1048576
  (2 shorter events, 0.0 us)
Async XLA Ops:
  0.7 0.7 copy-start.3
  0.7 0.7 copy-start.4
  1.4 0.7 copy-start
  1.4 0.7 copy-start.1
  2.1 0.7 copy-start.2
